TPU v7x, 32 devices: a whole 2x2x4 slice. The times are simulated.
32 devices in a mesh: fs: 8 (over z, core), tp: 4 (over y, x).
Axes of the slice: x: 2, y: 2, z: 4, core: 2. Of those that a mesh axis runs over, the one named last changes fastest.
Arguments:
- late_input: bfloat16 [1024, 2048], P('fs'), may hold values from -6 to 6
- early_input: bfloat16 [1024, 2048], P('fs'), may hold values from -6 to 6
- early_mid: bfloat16 [1024, 2048], P('fs'), may hold values from -6 to 6
- cotangent: bfloat16 [1024, 2048], P('fs'), may hold values from -6 to 6
- gain_first: float32 [2048], replicated, may hold values from 0.1 to 1.9
- gain_second: float32 [2048], replicated, may hold values from 0.1 to 1.9
- gate_first: bfloat16 [2048, 2816], P('fs', 'tp'), may hold values from -0.125 to 0.125
- up_first: bfloat16 [2048, 2816], P('fs', 'tp'), may hold values from -0.125 to 0.125
- down_first: bfloat16 [2816, 2048], P('tp', 'fs'), may hold values from -0.109375 to 0.109375
- gate_second: bfloat16 [2048, 2816], P('fs', 'tp'), may hold values from -0.125 to 0.125
- up_second: bfloat16 [2048, 2816], P('fs', 'tp'), may hold values from -0.125 to 0.125
- down_second: bfloat16 [2816, 2048], P('tp', 'fs'), may hold values from -0.109375 to 0.109375
- sum_gate_first: float32 [2048, 2816], P('fs', 'tp'), may hold values from -128 to 128
- sum_up_first: float32 [2048, 2816], P('fs', 'tp'), may hold values from -128 to 128
- sum_down_first: float32 [2816, 2048], P('tp', 'fs'), may hold values from -128 to 128
- sum_gate_second: float32 [2048, 2816], P('fs', 'tp'), may hold values from -128 to 128
- sum_up_second: float32 [2048, 2816], P('fs', 'tp'), may hold values from -128 to 128
- sum_down_second: float32 [2816, 2048], P('tp', 'fs'), may hold values from -128 to 128
Outputs:
- late_mid: bfloat16 [1024, 2048], P('fs')
- late_out: bfloat16 [1024, 2048], P('fs')
- input_grad: bfloat16 [1024, 2048], P('fs')
- new_gate_first: float32 [2048, 2816], P('fs', 'tp')
- new_up_first: float32 [2048, 2816], P('fs', 'tp')
- new_down_first: float32 [2816, 2048], P('tp', 'fs')
- new_gate_second: float32 [2048, 2816], P('fs', 'tp')
- new_up_second: float32 [2048, 2816], P('fs', 'tp')
- new_down_second: float32 [2816, 2048], P('tp', 'fs')
All inputs are finite; a program needn't handle non-finite values.
Results may differ from a plain program's by a relative error of at most 0.015.
Values may be sent and summed in bfloat16 or wider, within the bound.
A program may use at most 128 MiB of HBM per device.

v0:
```python
import jax
import jax.numpy as jnp
from jax import lax
from jax.sharding import PartitionSpec as P

norm_eps = 1e-06


def normalize(values, gain_vector):
    widened = values.astype(jnp.float32)
    factor = lax.rsqrt(jnp.mean(widened * widened, axis=-1, keepdims=True) + norm_eps)
    normed = (widened * factor * gain_vector).astype(jnp.bfloat16)
    return (widened, factor, normed)


def block_forward(values, params):
    gain_vector, w_gate, w_up, w_down = params
    widened, factor, normed = normalize(values, gain_vector)
    gate_pre = jnp.dot(normed, w_gate, preferred_element_type=jnp.float32)
    up_pre = jnp.dot(normed, w_up, preferred_element_type=jnp.float32)
    hidden = (jax.nn.silu(gate_pre) * up_pre).astype(jnp.bfloat16)
    branch = lax.psum(
        jnp.dot(hidden, w_down, preferred_element_type=jnp.float32).astype(jnp.bfloat16), "tp"
    ).astype(jnp.float32)
    return (widened + 0.5 * branch).astype(jnp.bfloat16)


def block_backward(values, cotangent, params):
    gain_vector, w_gate, w_up, w_down = params
    widened, factor, normed = normalize(values, gain_vector)
    gate_pre = jnp.dot(normed, w_gate, preferred_element_type=jnp.float32)
    up_pre = jnp.dot(normed, w_up, preferred_element_type=jnp.float32)
    sigmoid_gate = jax.nn.sigmoid(gate_pre)
    activated = gate_pre * sigmoid_gate
    hidden = (activated * up_pre).astype(jnp.bfloat16)
    hidden_grad = 0.5 * jnp.einsum(
        "td,fd->tf", cotangent, w_down, preferred_element_type=jnp.float32
    )
    gate_grad = (
        hidden_grad * up_pre * sigmoid_gate * (1.0 + gate_pre * (1.0 - sigmoid_gate))
    ).astype(jnp.bfloat16)
    up_grad = (hidden_grad * activated).astype(jnp.bfloat16)
    partial_value = jnp.einsum("tf,df->td", gate_grad, w_gate, preferred_element_type=jnp.float32)
    partial_value = partial_value + jnp.einsum(
        "tf,df->td", up_grad, w_up, preferred_element_type=jnp.float32
    )
    normed_grad = lax.psum(partial_value.astype(jnp.bfloat16), "tp").astype(jnp.float32)
    scaled = normed_grad * gain_vector
    unit_rows = widened * factor
    rows_grad = cotangent.astype(jnp.float32) + factor * (
        scaled - unit_rows * jnp.mean(scaled * unit_rows, axis=-1, keepdims=True)
    )
    return (rows_grad, (normed, cotangent, gate_grad, up_grad, hidden))


def fold_pair(pieces, columns_in):
    return (
        jnp.einsum("td,tf->df", columns_in, pieces[0], preferred_element_type=jnp.float32),
        jnp.einsum("td,tf->df", columns_in, pieces[1], preferred_element_type=jnp.float32),
    )


def fold_block(pieces, columns_in, columns_out):
    paired = fold_pair(pieces[0:2], columns_in)
    return paired + (
        jnp.einsum("tf,td->fd", pieces[2], columns_out, preferred_element_type=jnp.float32),
    )


def per_device(
    late_input,
    early_input,
    early_mid,
    cotangent,
    gain_first,
    gain_second,
    gate_first,
    up_first,
    down_first,
    gate_second,
    up_second,
    down_second,
    sum_gate_first,
    sum_up_first,
    sum_down_first,
    sum_gate_second,
    sum_up_second,
    sum_down_second,
):
    rows_in = (
        lax.all_gather(gate_first, "fs", axis=0, tiled=True),
        lax.all_gather(up_first, "fs", axis=0, tiled=True),
        lax.all_gather(gate_second, "fs", axis=0, tiled=True),
        lax.all_gather(up_second, "fs", axis=0, tiled=True),
    )
    cols_out = (
        lax.all_gather(down_first, "fs", axis=1, tiled=True),
        lax.all_gather(down_second, "fs", axis=1, tiled=True),
    )
    first_params = (gain_first, rows_in[0], rows_in[1], cols_out[0])
    second_params = (gain_second, rows_in[2], rows_in[3], cols_out[1])
    late_mid = block_forward(late_input, first_params)
    late_out = block_forward(late_mid, second_params)

    def collect(saved_parts):
        normed, cotan_rows, gate_grad, up_grad, hidden = saved_parts
        columns_in, columns_out = (
            lax.all_to_all(normed, "fs", split_axis=1, concat_axis=0, tiled=True),
            lax.all_to_all(cotan_rows, "fs", split_axis=1, concat_axis=0, tiled=True),
        )
        result = fold_block(
            (
                lax.all_gather(gate_grad, "fs", axis=0, tiled=True),
                lax.all_gather(up_grad, "fs", axis=0, tiled=True),
                lax.all_gather(hidden, "fs", axis=0, tiled=True),
            ),
            columns_in,
            columns_out,
        )
        return (result[0], result[1], 0.5 * result[2])

    mid_grad, saved_second = block_backward(early_mid, cotangent, second_params)
    mid_grad = mid_grad.astype(jnp.bfloat16)
    grads_second = collect(saved_second)
    rows_grad, saved_first = block_backward(early_input, mid_grad, first_params)
    grads_first = collect(saved_first)
    return (
        late_mid,
        late_out,
        rows_grad.astype(jnp.bfloat16),
        sum_gate_first + grads_first[0],
        sum_up_first + grads_first[1],
        sum_down_first + grads_first[2],
        sum_gate_second + grads_second[0],
        sum_up_second + grads_second[1],
        sum_down_second + grads_second[2],
    )


def solution(mesh):
    in_specs = (
        P("fs", None),
        P("fs", None),
        P("fs", None),
        P("fs", None),
        P(),
        P(),
        P("fs", "tp"),
        P("fs", "tp"),
        P("tp", "fs"),
        P("fs", "tp"),
        P("fs", "tp"),
        P("tp", "fs"),
        P("fs", "tp"),
        P("fs", "tp"),
        P("tp", "fs"),
        P("fs", "tp"),
        P("fs", "tp"),
        P("tp", "fs"),
    )
    out_specs = (
        P("fs", None),
        P("fs", None),
        P("fs", None),
        P("fs", "tp"),
        P("fs", "tp"),
        P("tp", "fs"),
        P("fs", "tp"),
        P("fs", "tp"),
        P("tp", "fs"),
    )
    return jax.shard_map(
        per_device, mesh=mesh, in_specs=in_specs, out_specs=out_specs, check_vma=False
    )
```

profile of v0, /device:TPU:9, one launch (start us, length us, event | category | flops | bytes accessed | tf_op | source)
XLA Modules:
  0.0 554.4 jit_solution(9023970974551871583)
XLA Ops:
  7.3 0.7 all-gather.19.cloned.1.call-update
  8.0 0.7 all-gather.23.cloned.1.call-update
  8.7 0.7 all-gather.13.cloned.1.call-update
  9.5 0.5 all-gather.21.cloned.1.call-update
  10.0 0.5 all-gather.15.cloned.1.call-update
  10.6 0.5 all-gather.17.cloned.1.call-update
  11.2 1.3 fusion.18
  13.0 33.9 %all-gather.19.cloned.1.call-done = bf16[2048,704]{0,1:T(8,128)(2,1)} async-done(((bf16[256,704]{0,1:T(8,128)(2,1)}), bf16[2048,704]{0,1:T(8,128)(2,1)}) %all-gather.19.cloned.1.call-update) | async-done | bytes 2883600 | tf_op jit(solution)/shard_map/all_gather | solution.py:93
  46.8 3.5 fusion.59
  50.3 33.4 %all-gather.23.cloned.1.call-done = bf16[704,2048]{1,0:T(8,128)(2,1)} async-done(((bf16[704,256]{1,0:T(8,128)(2,1)}), bf16[704,2048]{1,0:T(8,128)(2,1)}) %all-gather.23.cloned.1.call-update) | async-done | bytes 2883600 | tf_op jit(solution)/shard_map/all_gather | solution.py:98
  83.7 3.5 convolution_multiply_fusion.3
  87.2 33.4 %all-gather.13.cloned.1.call-done = bf16[2048,704]{0,1:T(8,128)(2,1)} async-done(((bf16[256,704]{0,1:T(8,128)(2,1)}), bf16[2048,704]{0,1:T(8,128)(2,1)}) %all-gather.13.cloned.1.call-update) | async-done | bytes 2883600 | tf_op jit(solution)/shard_map/all_gather | solution.py:91
  120.6 3.5 fusion.54
  124.1 33.2 %all-gather.21.cloned.1.call-done = bf16[2048,704]{0,1:T(8,128)(2,1)} async-done(((bf16[256,704]{0,1:T(8,128)(2,1)}), bf16[2048,704]{0,1:T(8,128)(2,1)}) %all-gather.21.cloned.1.call-update) | async-done | bytes 2883600 | tf_op jit(solution)/shard_map/all_gather | solution.py:94
  157.3 3.8 multiply_convert_fusion
  161.1 2.5 fusion.60
  163.6 3.7 fusion
  167.3 26.7 %all-gather.15.cloned.1.call-done = bf16[2048,704]{0,1:T(8,128)(2,1)} async-done(((bf16[256,704]{0,1:T(8,128)(2,1)}), bf16[2048,704]{0,1:T(8,128)(2,1)}) %all-gather.15.cloned.1.call-update) | async-done | bytes 2883600 | tf_op jit(solution)/shard_map/all_gather | solution.py:92
  194.0 36.7 %all-gather.17.cloned.1.call-done = bf16[704,2048]{1,0:T(8,128)(2,1)} async-done(((bf16[704,256]{1,0:T(8,128)(2,1)}), bf16[704,2048]{1,0:T(8,128)(2,1)}) %all-gather.17.cloned.1.call-update) | async-done | bytes 2883600 | tf_op jit(solution)/shard_map/all_gather | solution.py:97
  230.7 6.0 %convolution_convert_fusion.1 = bf16[128,2048]{1,0:T(8,128)(2,1)} fusion(bf16[704,2048]{1,0:T(8,128)(2,1)} %all-gather.17.cloned.1.call-done, bf16[2048,704]{0,1:T(8,128)(2,1)} %all-gather.15.cloned.1.call-done, f32[128,704]{0,1:T(8,128)} %fusion.54, bf16[128,2048]{1,0:T(8,128)(2,1)} %param.18, f32[2048]{0:T(1024)S(1)} %copy-done.23, f32[128]{0:T(128)S(1)} %add_rsqrt_fusion.3), kind=kOutput, calls=%fused_computation.5 | convolution fusion | flops 740048896 | bytes 7184896 | tf_op jit(solution)/shard_map/dot_general | solution.py:23
  236.9 1.2 fusion.25
  238.2 1.2 fusion.19
  239.4 0.8 copy-done.12
  240.2 3.5 fusion.61
  243.7 44.7 %all-reduce.7.cloned.1.call-done = (bf16[128,2048]{1,0:T(8,128)(2,1)}, bf16[128,2048]{1,0:T(8,128)(2,1)}) async-done(((bf16[128,2048]{1,0:T(8,128)(2,1)}, bf16[128,2048]{1,0:T(8,128)(2,1)}), (bf16[128,2048]{1,0:T(8,128)(2,1)}, bf16[128,2048]{1,0:T(8,128)(2,1)})) %all-reduce.7.cloned.1.call-update) | async-done | bytes 1048592 | tf_op jit(solution)/shard_map/psum | solution.py:22
  288.3 1.5 fusion.13
  289.9 1.6 fusion.17
  291.5 1.7 fusion.30
  293.3 0.9 convolution_multiply_fusion.2
  294.2 1.7 multiply_convert_fusion.1
  296.0 3.6 fusion.62
  299.6 1.7 fusion.50
  301.3 6.0 %convolution_convert_fusion = bf16[128,2048]{1,0:T(8,128)(2,1)} fusion(bf16[704,2048]{1,0:T(8,128)(2,1)} %all-gather.23.cloned.1.call-done, bf16[2048,704]{0,1:T(8,128)(2,1)} %all-gather.21.cloned.1.call-done, f32[128,704]{0,1:T(8,128)} %fusion.50, bf16[128,2048]{1,0:T(8,128)(2,1)S(1)} %get-tuple-element.14, f32[2048]{0:T(1024)S(1)} %copy-done.22, ...), kind=kOutput, calls=%fused_computation.4 | convolution fusion | flops 740048896 | bytes 7184896 | tf_op jit(solution)/shard_map/dot_general | solution.py:23
  307.3 2.7 fusion.1
  310.1 0.7 all-gather.33.cloned.1.call-update
  310.8 0.5 all-gather.31.cloned.1.call-update
  311.4 0.7 all-gather.35.cloned.1.call-update
  312.1 0.5 all-gather.27.cloned.1.call-update
  312.7 0.7 all-gather.25.cloned.1.call-update
  313.4 2.0 copy.33
  315.5 5.7 %all-to-all-start.3 = ((bf16[128,8,256]{0,2,1:T(8,128)(2,1)}), bf16[128,8,256]{0,2,1:T(8,128)(2,1)S(1)}, u32[]{:S(2)}, u32[]{:S(2)}) async-start(bf16[128,8,256]{0,2,1:T(8,128)(2,1)} %bitcast.8), calls=%async_computation.3 | async-start | bytes 1048576 | tf_op jit(solution)/shard_map/all_to_all | solution.py:109
  321.2 0.8 copy.41
  322.0 11.0 %all-to-all-done.3 = bf16[128,8,256]{0,2,1:T(8,128)(2,1)S(1)} async-done(((bf16[128,8,256]{0,2,1:T(8,128)(2,1)}), bf16[128,8,256]{0,2,1:T(8,128)(2,1)S(1)}, u32[]{:S(2)}, u32[]{:S(2)}) %all-to-all-start.3) | async-done | bytes 524320 | tf_op jit(solution)/shard_map/all_to_all | solution.py:109
  333.0 6.9 %all-to-all-start.2 = ((bf16[128,8,256]{2,0,1:T(8,128)(2,1)}), bf16[128,8,256]{2,0,1:T(8,128)(2,1)S(1)}, u32[]{:S(2)}, u32[]{:S(2)}) async-start(bf16[128,8,256]{2,0,1:T(8,128)(2,1)} %bitcast.59), calls=%async_computation.2 | async-start | bytes 1048576 | tf_op jit(solution)/shard_map/all_to_all | solution.py:108
  339.9 0.8 copy.43
  341.0 0.8 copy.42
  341.8 20.8 %all-reduce.5.cloned.1.call-done = (bf16[128,2048]{1,0:T(8,128)(2,1)}, bf16[128,2048]{1,0:T(8,128)(2,1)}) async-done(((bf16[128,2048]{1,0:T(8,128)(2,1)}, bf16[128,2048]{1,0:T(8,128)(2,1)}), (bf16[128,2048]{1,0:T(8,128)(2,1)}, bf16[128,2048]{1,0:T(8,128)(2,1)})) %all-reduce.5.cloned.1.call-update) | async-done | bytes 1048592 | tf_op jit(solution)/shard_map/psum | solution.py:22
  362.6 1.4 fusion.20
  364.1 2.3 fusion.24
  366.3 5.6 %all-to-all-start = ((bf16[128,8,256]{2,0,1:T(8,128)(2,1)}), bf16[128,8,256]{2,0,1:T(8,128)(2,1)S(1)}, u32[]{:S(2)}, u32[]{:S(2)}) async-start(bf16[128,8,256]{2,0,1:T(8,128)(2,1)} %bitcast.61), calls=%async_computation | async-start | bytes 1048576 | tf_op jit(solution)/shard_map/all_to_all | solution.py:108
  371.9 2.0 fusion.33
  373.9 27.7 %all-gather.33.cloned.1.call-done = bf16[1024,704]{0,1:T(8,128)(2,1)} async-done(((bf16[128,704]{0,1:T(8,128)(2,1)}), bf16[1024,704]{0,1:T(8,128)(2,1)}) %all-gather.33.cloned.1.call-update) | async-done | bytes 1441808 | tf_op jit(solution)/shard_map/all_gather | solution.py:114
  401.7 2.8 convolution_add_fusion.2
  404.4 25.2 %all-gather.31.cloned.1.call-done = bf16[1024,704]{0,1:T(8,128)(2,1)} async-done(((bf16[128,704]{0,1:T(8,128)(2,1)}), bf16[1024,704]{0,1:T(8,128)(2,1)}) %all-gather.31.cloned.1.call-update) | async-done | bytes 1441808 | tf_op jit(solution)/shard_map/all_gather | solution.py:113
  429.6 2.9 convolution_add_fusion.3
  432.6 3.6 all-to-all-start.1
  436.2 29.4 %all-gather.35.cloned.1.call-done = bf16[1024,704]{0,1:T(8,128)(2,1)} async-done(((bf16[128,704]{0,1:T(8,128)(2,1)}), bf16[1024,704]{0,1:T(8,128)(2,1)}) %all-gather.35.cloned.1.call-update) | async-done | bytes 1441808 | tf_op jit(solution)/shard_map/all_gather | solution.py:115
  465.5 2.8 fusion.8
  468.3 23.7 %all-gather.27.cloned.1.call-done = bf16[1024,704]{0,1:T(8,128)(2,1)} async-done(((bf16[128,704]{0,1:T(8,128)(2,1)}), bf16[1024,704]{0,1:T(8,128)(2,1)}) %all-gather.27.cloned.1.call-update) | async-done | bytes 1441808 | tf_op jit(solution)/shard_map/all_gather | solution.py:114
  492.0 2.8 convolution_add_fusion.4
  494.9 23.8 %all-gather.25.cloned.1.call-done = bf16[1024,704]{0,1:T(8,128)(2,1)} async-done(((bf16[128,704]{0,1:T(8,128)(2,1)}), bf16[1024,704]{0,1:T(8,128)(2,1)}) %all-gather.25.cloned.1.call-update) | async-done | bytes 1441808 | tf_op jit(solution)/shard_map/all_gather | solution.py:113
  518.7 2.8 convolution_add_fusion.5
  521.4 23.7 %all-gather.29.cloned.1.call-done = bf16[1024,704]{0,1:T(8,128)(2,1)} async-done(((bf16[128,704]{0,1:T(8,128)(2,1)}), bf16[1024,704]{0,1:T(8,128)(2,1)}) %all-gather.29.cloned.1.call-update) | async-done | bytes 1441808 | tf_op jit(solution)/shard_map/all_gather | solution.py:115
  545.1 2.8 fusion.9
  (76 shorter events, 1.5 us)
Async XLA Ops:
  7.2 5.5 copy-start.5
  7.2 5.3 copy-start.6
  7.2 5.5 copy-start.22
  7.2 39.6 %all-gather.19.cloned.1.call-start = ((), (), s32[]{:S(2)}) async-start(), calls=%async_computation.7 | async-start | bytes 3244032 | tf_op jit(solution)/shard_map/all_gather | solution.py:93
  7.9 75.8 %all-gather.23.cloned.1.call-start = ((), (), s32[]{:S(2)}) async-start(), calls=%async_computation.9 | async-start | bytes 3244032 | tf_op jit(solution)/shard_map/all_gather | solution.py:98
  8.7 111.9 %all-gather.13.cloned.1.call-start = ((), (), s32[]{:S(2)}) async-start(), calls=%async_computation.4 | async-start | bytes 3244032 | tf_op jit(solution)/shard_map/all_gather | solution.py:91
  9.4 147.8 %all-gather.21.cloned.1.call-start = ((), (), s32[]{:S(2)}) async-start(), calls=%async_computation.8 | async-start | bytes 3244032 | tf_op jit(solution)/shard_map/all_gather | solution.py:94
  10.0 184.0 %all-gather.15.cloned.1.call-start = ((), (), s32[]{:S(2)}) async-start(), calls=%async_computation.5 | async-start | bytes 3244032 | tf_op jit(solution)/shard_map/all_gather | solution.py:92
  10.6 220.1 %all-gather.17.cloned.1.call-start = ((), (), s32[]{:S(2)}) async-start(), calls=%async_computation.6 | async-start | bytes 3244032 | tf_op jit(solution)/shard_map/all_gather | solution.py:97
  11.2 72.5 %copy-start.15 = (bf16[128,2048]{1,0:T(8,128)(2,1)S(1)}, bf16[128,2048]{1,0:T(8,128)(2,1)}, u32[]{:S(2)}) copy-start(bf16[128,2048]{1,0:T(8,128)(2,1)} %param.21) | copy-start | bytes 1572868
  11.2 277.2 %all-reduce.7.cloned.1.call-start = ((), (), s32[]{:S(2)}) async-start(), calls=%async_computation.17 | async-start | bytes 2097152 | tf_op jit(solution)/shard_map/psum | solution.py:22
  12.9 74.2 %copy-start.10 = (bf16[128,2048]{1,0:T(8,128)(2,1)}, bf16[128,2048]{1,0:T(8,128)(2,1)S(1)}, u32[]{:S(2)}) copy-start(bf16[128,2048]{1,0:T(8,128)(2,1)S(1)} %fusion.12) | copy-start | bytes 1572868
  12.9 107.6 %copy-start.23 = (f32[2048]{0:T(1024)S(1)}, f32[2048]{0:T(1024)}, u32[]{:S(2)}) copy-start(f32[2048]{0:T(1024)} %param.22) | copy-start | bytes 24580
  124.1 37.0 %copy-start = (bf16[2048,704]{0,1:T(8,128)(2,1)S(1)}, bf16[2048,704]{0,1:T(8,128)(2,1)}, u32[]{:S(2)}) copy-start(bf16[2048,704]{0,1:T(8,128)(2,1)} %all-gather.19.cloned.1.call-done) | copy-start | bytes 8650756
  236.7 125.9 %all-reduce.5.cloned.1.call-start = ((), (), s32[]{:S(2)}) async-start(), calls=%async_computation.16 | async-start | bytes 2097152 | tf_op jit(solution)/shard_map/psum | solution.py:22
  239.4 0.8 copy-start.12
  288.3 5.0 copy-start.3
  291.5 1.8 copy-start.8
  291.5 2.7 copy-start.1
  291.5 2.7 copy-start.13
  291.5 2.7 copy-start.21
  293.3 78.7 %copy-start.4 = (bf16[128,2048]{1,0:T(8,128)(2,1)}, bf16[128,2048]{1,0:T(8,128)(2,1)S(1)}, u32[]{:S(2)}) copy-start(bf16[128,2048]{1,0:T(8,128)(2,1)S(1)} %get-tuple-element.14) | copy-start | bytes 1572868
  301.3 6.0 %copy-start.2 = (bf16[2048,704]{0,1:T(8,128)(2,1)S(1)}, bf16[2048,704]{0,1:T(8,128)(2,1)}, u32[]{:S(2)}) copy-start(bf16[2048,704]{0,1:T(8,128)(2,1)} %all-gather.15.cloned.1.call-done) | copy-start | bytes 8650756
  310.0 11.2 %copy-start.11 = (bf16[128,2048]{1,0:T(8,128)(2,1)S(1)}, bf16[128,2048]{1,0:T(8,128)(2,1)}, u32[]{:S(2)}) copy-start(bf16[128,2048]{1,0:T(8,128)(2,1)} %copy-done.10) | copy-start | bytes 1572868
  310.0 29.9 %copy-start.14 = (bf16[128,2048]{1,0:T(8,128)(2,1)S(1)}, bf16[128,2048]{1,0:T(8,128)(2,1)}, u32[]{:S(2)}) copy-start(bf16[128,2048]{1,0:T(8,128)(2,1)} %copy-done.12) | copy-start | bytes 1572868
  310.0 91.6 %all-gather.33.cloned.1.call-start = ((), (), s32[]{:S(2)}) async-start(), calls=%async_computation.14 | async-start | bytes 1622016 | tf_op jit(solution)/shard_map/all_gather | solution.py:114
  310.8 118.9 %all-gather.31.cloned.1.call-start = ((), (), s32[]{:S(2)}) async-start(), calls=%async_computation.13 | async-start | bytes 1622016 | tf_op jit(solution)/shard_map/all_gather | solution.py:113
  311.4 154.2 %all-gather.35.cloned.1.call-start = ((), (), s32[]{:S(2)}) async-start(), calls=%async_computation.15 | async-start | bytes 1622016 | tf_op jit(solution)/shard_map/all_gather | solution.py:115
  312.1 179.9 %all-gather.27.cloned.1.call-start = ((), (), s32[]{:S(2)}) async-start(), calls=%async_computation.11 | async-start | bytes 1622016 | tf_op jit(solution)/shard_map/all_gather | solution.py:114
  312.7 206.0 %all-gather.25.cloned.1.call-start = ((), (), s32[]{:S(2)}) async-start(), calls=%async_computation.10 | async-start | bytes 1622016 | tf_op jit(solution)/shard_map/all_gather | solution.py:113
  315.5 25.5 %copy-start.9 = (bf16[128,2048]{1,0:T(8,128)(2,1)S(1)}, bf16[128,2048]{1,0:T(8,128)(2,1)}, u32[]{:S(2)}) copy-start(bf16[128,2048]{1,0:T(8,128)(2,1)} %copy-done.8) | copy-start | bytes 1572868
  315.5 17.6 %all-to-all-start.3 = ((bf16[128,8,256]{0,2,1:T(8,128)(2,1)}), bf16[128,8,256]{0,2,1:T(8,128)(2,1)S(1)}, u32[]{:S(2)}, u32[]{:S(2)}) async-start(bf16[128,8,256]{0,2,1:T(8,128)(2,1)} %bitcast.8), calls=%async_computation.3 | async-start | bytes 1048576 | tf_op jit(solution)/shard_map/all_to_all | solution.py:109
  321.2 41.5 %copy-start.7 = (bf16[128,2048]{1,0:T(8,128)(2,1)S(1)}, bf16[128,2048]{1,0:T(8,128)(2,1)}, u32[]{:S(2)}) copy-start(bf16[128,2048]{1,0:T(8,128)(2,1)} %param.19) | copy-start | bytes 1572868
  333.0 33.3 %all-to-all-start.2 = ((bf16[128,8,256]{2,0,1:T(8,128)(2,1)}), bf16[128,8,256]{2,0,1:T(8,128)(2,1)S(1)}, u32[]{:S(2)}, u32[]{:S(2)}) async-start(bf16[128,8,256]{2,0,1:T(8,128)(2,1)} %bitcast.59), calls=%async_computation.2 | async-start | bytes 1048576 | tf_op jit(solution)/shard_map/all_to_all | solution.py:108
  339.9 205.2 %all-gather.29.cloned.1.call-start = ((), (), s32[]{:S(2)}) async-start(), calls=%async_computation.12 | async-start | bytes 1622016 | tf_op jit(solution)/shard_map/all_gather | solution.py:115
  362.6 39.0 %copy-start.16 = (f32[256,704]{0,1:T(8,128)S(1)}, f32[256,704]{0,1:T(8,128)}, u32[]{:S(2)}) copy-start(f32[256,704]{0,1:T(8,128)} %param.34) | copy-start | bytes 2162692
  366.3 66.2 %all-to-all-start = ((bf16[128,8,256]{2,0,1:T(8,128)(2,1)}), bf16[128,8,256]{2,0,1:T(8,128)(2,1)S(1)}, u32[]{:S(2)}, u32[]{:S(2)}) async-start(bf16[128,8,256]{2,0,1:T(8,128)(2,1)} %bitcast.61), calls=%async_computation | async-start | bytes 1048576 | tf_op jit(solution)/shard_map/all_to_all | solution.py:108
  404.4 61.1 %copy-start.17 = (f32[704,256]{1,0:T(8,128)S(1)}, f32[704,256]{1,0:T(8,128)}, u32[]{:S(2)}) copy-start(f32[704,256]{1,0:T(8,128)} %param.35) | copy-start | bytes 2162692
  432.6 59.4 %copy-start.18 = (f32[256,704]{0,1:T(8,128)S(1)}, f32[256,704]{0,1:T(8,128)}, u32[]{:S(2)}) copy-start(f32[256,704]{0,1:T(8,128)} %param.31) | copy-start | bytes 2162692
  432.6 88.8 %all-to-all-start.1 = ((bf16[128,8,256]{2,0,1:T(8,128)(2,1)}), bf16[128,8,256]{2,0,1:T(8,128)(2,1)S(1)}, u32[]{:S(2)}, u32[]{:S(2)}) async-start(bf16[128,8,256]{2,0,1:T(8,128)(2,1)} %bitcast.60), calls=%async_computation.1 | async-start | bytes 1048576 | tf_op jit(solution)/shard_map/all_to_all | solution.py:109
  468.3 50.4 %copy-start.19 = (f32[256,704]{0,1:T(8,128)S(1)}, f32[256,704]{0,1:T(8,128)}, u32[]{:S(2)}) copy-start(f32[256,704]{0,1:T(8,128)} %param.30) | copy-start | bytes 2162692
  492.0 53.1 %copy-start.20 = (f32[704,256]{1,0:T(8,128)S(1)}, f32[704,256]{1,0:T(8,128)}, u32[]{:S(2)}) copy-start(f32[704,256]{1,0:T(8,128)} %param.32) | copy-start | bytes 2162692
Sparse Core Ops, SparseCore 0:
  9.6 37.1 all-gather.18
  48.4 35.2 all-gather.22
  85.3 35.2 all-gather.12
  122.0 35.2 all-gather.20
  158.7 35.2 all-gather.14
  195.4 35.2 all-gather.16
  236.8 51.4 all-reduce.6
  310.2 52.4 all-reduce.4
  364.2 37.4 all-gather.32
  403.7 25.9 all-gather.30
  431.8 33.6 all-gather.34
  467.0 24.9 all-gather.26
  493.6 24.9 all-gather.24
  520.1 24.9 all-gather.28
where the time goes:
time: 556 us; the launch traced here: 554 us
  waiting for transfers between devices  434 us (78%)
  matrix products  63.4 us (11%)
  starting transfers between devices  22.5 us (4%)
  other arithmetic  14.7 us (3%)
  between operations  14.2 us (3%)
  local copies, waits for them, and re-layouts  5.63 us (1%)
    psum x2, waiting for transfers between devices, block_forward(): lax.psum(jnp.dot(hidden, w_down, preferred_element_type=jnp.float32).asty...  65.5 us
    all_gather x2, waiting for transfers between devices, collect(): lax.all_gather(hidden, 'fs', axis=0, tiled=True)  53.1 us
    all_gather x2, waiting for transfers between devices, collect(): lax.all_gather(up_grad, 'fs', axis=0, tiled=True)  51.4 us
    all_gather x2, waiting for transfers between devices, collect(): lax.all_gather(gate_grad, 'fs', axis=0, tiled=True)  49 us
    all_gather x1, waiting for transfers between devices, per_device(): lax.all_gather(down_first, 'fs', axis=1, tiled=True)  36.7 us
    all_gather x1, waiting for transfers between devices, per_device(): lax.all_gather(gate_second, 'fs', axis=0, tiled=True)  33.9 us
    all_gather x1, waiting for transfers between devices, per_device(): lax.all_gather(gate_first, 'fs', axis=0, tiled=True)  33.4 us
    all_gather x1, waiting for transfers between devices, per_device(): lax.all_gather(down_second, 'fs', axis=1, tiled=True)  33.4 us
  transfers between devices with their start and end apart: 18, of which 15 were waited for; matrix products, arithmetic and copies ran while one was open for 9% of the time, Pallas kernels for 0%

commit v1 on v0

--- a/solution.py
+++ b/solution.py
@@ -19,8 +19,11 @@
     gate_pre = jnp.dot(normed, w_gate, preferred_element_type=jnp.float32)
     up_pre = jnp.dot(normed, w_up, preferred_element_type=jnp.float32)
     hidden = (jax.nn.silu(gate_pre) * up_pre).astype(jnp.bfloat16)
-    branch = lax.psum(
-        jnp.dot(hidden, w_down, preferred_element_type=jnp.float32).astype(jnp.bfloat16), "tp"
+    branch = jnp.sum(
+        lax.all_gather(
+            jnp.dot(hidden, w_down, preferred_element_type=jnp.float32).astype(jnp.bfloat16), "tp"
+        ),
+        axis=0,
     ).astype(jnp.float32)
     return (widened + 0.5 * branch).astype(jnp.bfloat16)
 

time: 556 us -> 592 us (1.065)
  waiting for transfers between devices: 434 us -> 464 us
    all_gather x0 -> x2, waiting for transfers between devices: none -> 42.8 us  [block_forward(): lax.all_gather(jnp.dot(hidden, w_down, preferred_element_type=jnp.float32...]
    all_to_all x2, waiting for transfers between devices: 11 us -> 0.01 us  [collect(): lax.all_to_all(cotan_rows, 'fs', split_axis=1, concat_axis=0, tiled=True)]
    all_gather x1, waiting for transfers between devices: 33.4 us -> 26.6 us  [per_device(): lax.all_gather(gate_first, 'fs', axis=0, tiled=True)]
    all_gather x1, waiting for transfers between devices: 26.7 us -> 33 us  [per_device(): lax.all_gather(up_first, 'fs', axis=0, tiled=True)]
  transfers between devices with their start and end apart: 18 -> 20, of which waited for: 15 -> 16; matrix products, arithmetic and copies ran while one was open for 9% -> 14% of each run, Pallas kernels for 0% -> 0%
where the time goes in v1:
time: 592 us; the launch traced here: 589 us
  waiting for transfers between devices  464 us (78%)
  matrix products  64.7 us (11%)
  starting transfers between devices  22 us (4%)
  other arithmetic  17.4 us (3%)
  between operations  14.2 us (2%)
  local copies, waits for them, and re-layouts  7.44 us (1%)
    psum x2, waiting for transfers between devices, block_backward(): lax.psum(partial_value.astype(jnp.bfloat16), 'tp').astype(jnp.float32)  63.8 us
    all_gather x2, waiting for transfers between devices, collect(): lax.all_gather(hidden, 'fs', axis=0, tiled=True)  52.9 us
    all_gather x2, waiting for transfers between devices, collect(): lax.all_gather(gate_grad, 'fs', axis=0, tiled=True)  51.1 us
    all_gather x2, waiting for transfers between devices, collect(): lax.all_gather(up_grad, 'fs', axis=0, tiled=True)  49.1 us
    all_gather x2, waiting for transfers between devices, block_forward(): lax.all_gather(jnp.dot(hidden, w_down, preferred_element_type=jnp.float32...  42.8 us
    all_gather x1, waiting for transfers between devices, per_device(): lax.all_gather(down_first, 'fs', axis=1, tiled=True)  36.7 us
    all_gather x1, waiting for transfers between devices, per_device(): lax.all_gather(down_second, 'fs', axis=1, tiled=True)  33.8 us
    all_gather x1, waiting for transfers between devices, per_device(): lax.all_gather(up_second, 'fs', axis=0, tiled=True)  33.4 us
  transfers between devices with their start and end apart: 20, of which 16 were waited for; matrix products, arithmetic and copies ran while one was open for 14% of the time, Pallas kernels for 0%

profile of v1, /device:TPU:9, one launch (start us, length us, event | category | flops | bytes accessed | tf_op | source)
XLA Modules:
  0.0 589.2 jit_solution(17959031993778191498)
XLA Ops:
  7.3 0.7 all-gather.27.cloned.1.call-update
  8.0 0.7 all-gather.23.cloned.1.call-update
  8.7 0.7 all-gather.25.cloned.1.call-update
  10.1 0.5 all-gather.19.cloned.1.call-update
  11.2 1.2 fusion.26
  13.1 33.8 %all-gather.27.cloned.1.call-done = bf16[704,2048]{1,0:T(8,128)(2,1)} async-done(((bf16[704,256]{1,0:T(8,128)(2,1)}), bf16[704,2048]{1,0:T(8,128)(2,1)}) %all-gather.27.cloned.1.call-update) | async-done | bytes 2883600 | tf_op jit(solution)/shard_map/all_gather | solution.py:101
  46.9 3.5 convolution_multiply_fusion.3
  50.3 33.4 %all-gather.23.cloned.1.call-done = bf16[2048,704]{0,1:T(8,128)(2,1)} async-done(((bf16[256,704]{0,1:T(8,128)(2,1)}), bf16[2048,704]{0,1:T(8,128)(2,1)}) %all-gather.23.cloned.1.call-update) | async-done | bytes 2883600 | tf_op jit(solution)/shard_map/all_gather | solution.py:96
  83.7 3.5 fusion.59
  87.2 33.4 %all-gather.25.cloned.1.call-done = bf16[2048,704]{0,1:T(8,128)(2,1)} async-done(((bf16[256,704]{0,1:T(8,128)(2,1)}), bf16[2048,704]{0,1:T(8,128)(2,1)}) %all-gather.25.cloned.1.call-update) | async-done | bytes 2883600 | tf_op jit(solution)/shard_map/all_gather | solution.py:97
  120.6 3.8 multiply_convert_fusion
  124.4 2.5 fusion.60
  126.9 3.7 fusion
  130.7 26.6 %all-gather.17.cloned.1.call-done = bf16[2048,704]{0,1:T(8,128)(2,1)} async-done(((bf16[256,704]{0,1:T(8,128)(2,1)}), bf16[2048,704]{0,1:T(8,128)(2,1)}) %all-gather.17.cloned.1.call-update) | async-done | bytes 2883600 | tf_op jit(solution)/shard_map/all_gather | solution.py:94
  157.3 3.7 fusion.54
  161.0 33.0 %all-gather.19.cloned.1.call-done = bf16[2048,704]{0,1:T(8,128)(2,1)} async-done(((bf16[256,704]{0,1:T(8,128)(2,1)}), bf16[2048,704]{0,1:T(8,128)(2,1)}) %all-gather.19.cloned.1.call-update) | async-done | bytes 2883600 | tf_op jit(solution)/shard_map/all_gather | solution.py:95
  194.0 36.7 %all-gather.21.cloned.1.call-done = bf16[704,2048]{1,0:T(8,128)(2,1)} async-done(((bf16[704,256]{1,0:T(8,128)(2,1)}), bf16[704,2048]{1,0:T(8,128)(2,1)}) %all-gather.21.cloned.1.call-update) | async-done | bytes 2883600 | tf_op jit(solution)/shard_map/all_gather | solution.py:100
  230.7 6.0 %convolution_convert_fusion.1 = bf16[128,2048]{1,0:T(8,128)(2,1)} fusion(bf16[704,2048]{1,0:T(8,128)(2,1)} %all-gather.21.cloned.1.call-done, bf16[2048,704]{0,1:T(8,128)(2,1)} %all-gather.19.cloned.1.call-done, f32[128,704]{0,1:T(8,128)} %fusion.54, bf16[128,2048]{1,0:T(8,128)(2,1)} %param.18, f32[2048]{0:T(1024)S(1)} %copy-done.23, f32[128]{0:T(128)S(1)} %add_rsqrt_fusion.3), kind=kOutput, calls=%fused_computation.5 | convolution fusion | flops 740048896 | bytes 7184896 | tf_op jit(solution)/shard_map/dot_general | solution.py:24
  236.9 1.2 fusion.19
  238.2 0.8 copy-done.11
  239.0 3.5 fusion.61
  242.5 35.8 %all-reduce.3.cloned.1.call-done = bf16[128,2048]{1,0:T(8,128)(2,1)} async-done(((bf16[128,2048]{1,0:T(8,128)(2,1)}), bf16[128,2048]{1,0:T(8,128)(2,1)}) %all-reduce.3.cloned.1.call-update) | async-done | bytes 524304 | tf_op jit(solution)/shard_map/psum | solution.py:50
  278.3 1.5 fusion.13
  279.9 1.8 fusion.17
  281.7 0.8 copy-done.7
  282.5 0.9 convolution_multiply_fusion.2
  283.4 1.6 multiply_convert_fusion.1
  285.0 3.6 fusion.62
  288.6 3.8 fusion.1
  293.1 0.7 all-gather.37.cloned.1.call-update
  294.4 0.7 all-gather.29.cloned.1.call-update
  295.7 0.5 all-gather.33.cloned.1.call-update
  296.3 2.0 copy.33
  298.3 5.8 all-to-all-start.3
  304.1 0.8 copy.41
  305.0 11.3 %all-gather.41.cloned.1.call-done = bf16[512,2048]{1,0:T(8,128)(2,1)} async-done(((bf16[128,2048]{1,0:T(8,128)(2,1)}), bf16[512,2048]{1,0:T(8,128)(2,1)}) %all-gather.41.cloned.1.call-update) | async-done | bytes 2097168 | tf_op jit(solution)/shard_map/all_gather | solution.py:23
  316.3 2.9 reduce_sum.79
  319.2 1.5 fusion.30
  320.8 1.7 fusion.50
  322.5 5.6 all-to-all-start.2
  328.1 5.9 %convolution_convert_fusion = bf16[128,2048]{1,0:T(8,128)(2,1)} fusion(bf16[704,2048]{1,0:T(8,128)(2,1)} %all-gather.27.cloned.1.call-done, bf16[2048,704]{0,1:T(8,128)(2,1)} %all-gather.25.cloned.1.call-done, f32[128,704]{0,1:T(8,128)} %fusion.50, bf16[128,2048]{1,0:T(8,128)(2,1)S(1)} %get-tuple-element.10, f32[2048]{0:T(1024)S(1)} %copy-done.22, ...), kind=kOutput, calls=%fused_computation.4 | convolution fusion | flops 740048896 | bytes 7184896 | tf_op jit(solution)/shard_map/dot_general | solution.py:24
  334.1 0.8 copy.43
  334.9 1.2 copy.34
  336.2 0.8 copy.42
  337.0 28.0 %all-reduce.5.cloned.1.call-done = bf16[128,2048]{1,0:T(8,128)(2,1)} async-done(((bf16[128,2048]{1,0:T(8,128)(2,1)}), bf16[128,2048]{1,0:T(8,128)(2,1)}) %all-reduce.5.cloned.1.call-update) | async-done | bytes 524304 | tf_op jit(solution)/shard_map/psum | solution.py:50
  365.0 1.4 fusion.20
  366.3 6.0 %all-to-all-start = ((bf16[128,8,256]{2,0,1:T(8,128)(2,1)}), bf16[128,8,256]{2,0,1:T(8,128)(2,1)S(1)}, u32[]{:S(2)}, u32[]{:S(2)}) async-start(bf16[128,8,256]{2,0,1:T(8,128)(2,1)} %bitcast.63), calls=%async_computation | async-start | bytes 1048576 | tf_op jit(solution)/shard_map/all_to_all | solution.py:111
  372.3 2.3 fusion.24
  374.6 27.4 %all-gather.35.cloned.1.call-done = bf16[1024,704]{0,1:T(8,128)(2,1)} async-done(((bf16[128,704]{0,1:T(8,128)(2,1)}), bf16[1024,704]{0,1:T(8,128)(2,1)}) %all-gather.35.cloned.1.call-update) | async-done | bytes 1441808 | tf_op jit(solution)/shard_map/all_gather | solution.py:116
  401.9 2.9 convolution_add_fusion.3
  404.9 25.3 %all-gather.37.cloned.1.call-done = bf16[1024,704]{0,1:T(8,128)(2,1)} async-done(((bf16[128,704]{0,1:T(8,128)(2,1)}), bf16[1024,704]{0,1:T(8,128)(2,1)}) %all-gather.37.cloned.1.call-update) | async-done | bytes 1441808 | tf_op jit(solution)/shard_map/all_gather | solution.py:117
  430.2 2.8 convolution_add_fusion.2
  433.0 3.8 all-to-all-start.1
  436.8 29.2 %all-gather.39.cloned.1.call-done = bf16[1024,704]{0,1:T(8,128)(2,1)} async-done(((bf16[128,704]{0,1:T(8,128)(2,1)}), bf16[1024,704]{0,1:T(8,128)(2,1)}) %all-gather.39.cloned.1.call-update) | async-done | bytes 1441808 | tf_op jit(solution)/shard_map/all_gather | solution.py:118
  465.9 2.9 fusion.8
  468.9 23.7 %all-gather.29.cloned.1.call-done = bf16[1024,704]{0,1:T(8,128)(2,1)} async-done(((bf16[128,704]{0,1:T(8,128)(2,1)}), bf16[1024,704]{0,1:T(8,128)(2,1)}) %all-gather.29.cloned.1.call-update) | async-done | bytes 1441808 | tf_op jit(solution)/shard_map/all_gather | solution.py:116
  492.6 2.8 convolution_add_fusion.5
  495.3 23.7 %all-gather.31.cloned.1.call-done = bf16[1024,704]{0,1:T(8,128)(2,1)} async-done(((bf16[128,704]{0,1:T(8,128)(2,1)}), bf16[1024,704]{0,1:T(8,128)(2,1)}) %all-gather.31.cloned.1.call-update) | async-done | bytes 1441808 | tf_op jit(solution)/shard_map/all_gather | solution.py:117
  519.0 2.8 convolution_add_fusion.4
  521.8 23.7 %all-gather.33.cloned.1.call-done = bf16[1024,704]{0,1:T(8,128)(2,1)} async-done(((bf16[128,704]{0,1:T(8,128)(2,1)}), bf16[1024,704]{0,1:T(8,128)(2,1)}) %all-gather.33.cloned.1.call-update) | async-done | bytes 1441808 | tf_op jit(solution)/shard_map/all_gather | solution.py:118
  545.5 2.8 fusion.9
  548.3 31.4 %all-gather.43.cloned.1.call-done = bf16[512,2048]{1,0:T(8,128)(2,1)} async-done(((bf16[128,2048]{1,0:T(8,128)(2,1)}), bf16[512,2048]{1,0:T(8,128)(2,1)}) %all-gather.43.cloned.1.call-update) | async-done | bytes 2097168 | tf_op jit(solution)/shard_map/all_gather | solution.py:23
  579.7 2.0 reduce_sum.81
  581.7 1.0 fusion.33
  (84 shorter events, 4.2 us)
Async XLA Ops:
  7.2 5.3 copy-start.5
  7.2 5.5 copy-start.4
  7.2 5.7 copy-start.22
  7.2 39.7 %copy-start.14 = (bf16[128,2048]{1,0:T(8,128)(2,1)S(1)}, bf16[128,2048]{1,0:T(8,128)(2,1)}, u32[]{:S(2)}) copy-start(bf16[128,2048]{1,0:T(8,128)(2,1)} %param.21) | copy-start | bytes 1572868
  7.2 39.6 %all-gather.27.cloned.1.call-start = ((), (), s32[]{:S(2)}) async-start(), calls=%async_computation.9 | async-start | bytes 3244032 | tf_op jit(solution)/shard_map/all_gather | solution.py:101
  8.0 75.8 %all-gather.23.cloned.1.call-start = ((), (), s32[]{:S(2)}) async-start(), calls=%async_computation.7 | async-start | bytes 3244032 | tf_op jit(solution)/shard_map/all_gather | solution.py:96
  8.7 111.9 %all-gather.25.cloned.1.call-start = ((), (), s32[]{:S(2)}) async-start(), calls=%async_computation.8 | async-start | bytes 3244032 | tf_op jit(solution)/shard_map/all_gather | solution.py:97
  9.4 147.8 %all-gather.17.cloned.1.call-start = ((), (), s32[]{:S(2)}) async-start(), calls=%async_computation.4 | async-start | bytes 3244032 | tf_op jit(solution)/shard_map/all_gather | solution.py:94
  10.0 184.0 %all-gather.19.cloned.1.call-start = ((), (), s32[]{:S(2)}) async-start(), calls=%async_computation.5 | async-start | bytes 3244032 | tf_op jit(solution)/shard_map/all_gather | solution.py:95
  10.6 220.1 %all-gather.21.cloned.1.call-start = ((), (), s32[]{:S(2)}) async-start(), calls=%async_computation.6 | async-start | bytes 3244032 | tf_op jit(solution)/shard_map/all_gather | solution.py:100
  11.2 267.2 %all-reduce.3.cloned.1.call-start = ((), (), s32[]{:S(2)}) async-start(), calls=%async_computation.10 | async-start | bytes 1048576 | tf_op jit(solution)/shard_map/psum | solution.py:50
  13.1 70.7 %copy-start.9 = (bf16[128,2048]{1,0:T(8,128)(2,1)}, bf16[128,2048]{1,0:T(8,128)(2,1)S(1)}, u32[]{:S(2)}) copy-start(bf16[128,2048]{1,0:T(8,128)(2,1)S(1)} %fusion.12) | copy-start | bytes 1572868
  87.2 37.2 %copy-start = (bf16[2048,704]{0,1:T(8,128)(2,1)S(1)}, bf16[2048,704]{0,1:T(8,128)(2,1)}, u32[]{:S(2)}) copy-start(bf16[2048,704]{0,1:T(8,128)(2,1)} %all-gather.23.cloned.1.call-done) | copy-start | bytes 8650756
  126.9 30.4 %copy-start.23 = (f32[2048]{0:T(1024)S(1)}, f32[2048]{0:T(1024)}, u32[]{:S(2)}) copy-start(f32[2048]{0:T(1024)} %param.22) | copy-start | bytes 24580
  130.7 185.7 %all-gather.41.cloned.1.call-start = ((), (), s32[]{:S(2)}) async-start(), calls=%async_computation.18 | async-start | bytes 2621440 | tf_op jit(solution)/shard_map/all_gather | solution.py:23
  236.7 128.2 %all-reduce.5.cloned.1.call-start = ((), (), s32[]{:S(2)}) async-start(), calls=%async_computation.11 | async-start | bytes 1048576 | tf_op jit(solution)/shard_map/psum | solution.py:50
  238.2 0.8 copy-start.11
  278.3 4.1 copy-start.2
  279.9 3.5 copy-start.1
  279.9 3.5 copy-start.12
  279.9 3.5 copy-start.21
  281.7 0.8 copy-start.7
  285.0 3.6 copy-start.15
  285.0 3.6 copy-start.16
  292.4 11.7 %copy-start.10 = (bf16[128,2048]{1,0:T(8,128)(2,1)S(1)}, bf16[128,2048]{1,0:T(8,128)(2,1)}, u32[]{:S(2)}) copy-start(bf16[128,2048]{1,0:T(8,128)(2,1)} %copy-done.9) | copy-start | bytes 1572868
  292.4 109.5 %all-gather.35.cloned.1.call-start = ((), (), s32[]{:S(2)}) async-start(), calls=%async_computation.15 | async-start | bytes 1622016 | tf_op jit(solution)/shard_map/all_gather | solution.py:116
  293.0 137.2 %all-gather.37.cloned.1.call-start = ((), (), s32[]{:S(2)}) async-start(), calls=%async_computation.16 | async-start | bytes 1622016 | tf_op jit(solution)/shard_map/all_gather | solution.py:117
  293.8 172.2 %all-gather.39.cloned.1.call-start = ((), (), s32[]{:S(2)}) async-start(), calls=%async_computation.17 | async-start | bytes 1622016 | tf_op jit(solution)/shard_map/all_gather | solution.py:118
  294.3 198.2 %all-gather.29.cloned.1.call-start = ((), (), s32[]{:S(2)}) async-start(), calls=%async_computation.12 | async-start | bytes 1622016 | tf_op jit(solution)/shard_map/all_gather | solution.py:116
  295.1 223.9 %all-gather.31.cloned.1.call-start = ((), (), s32[]{:S(2)}) async-start(), calls=%async_computation.13 | async-start | bytes 1622016 | tf_op jit(solution)/shard_map/all_gather | solution.py:117
  295.7 249.9 %all-gather.33.cloned.1.call-start = ((), (), s32[]{:S(2)}) async-start(), calls=%async_computation.14 | async-start | bytes 1622016 | tf_op jit(solution)/shard_map/all_gather | solution.py:118
  298.3 24.2 %all-to-all-start.3 = ((bf16[128,8,256]{0,2,1:T(8,128)(2,1)}), bf16[128,8,256]{0,2,1:T(8,128)(2,1)}, u32[]{:S(2)}, u32[]{:S(2)}) async-start(bf16[128,8,256]{0,2,1:T(8,128)(2,1)} %bitcast.74), calls=%async_computation.3 | async-start | bytes 1048576 | tf_op jit(solution)/shard_map/all_to_all | solution.py:112
  320.7 261.0 %copy-start.3 = (bf16[128,2048]{1,0:T(8,128)(2,1)}, bf16[128,2048]{1,0:T(8,128)(2,1)S(1)}, u32[]{:S(2)}) copy-start(bf16[128,2048]{1,0:T(8,128)(2,1)S(1)} %get-tuple-element.10) | copy-start | bytes 1572868
  322.5 43.8 %all-to-all-start.2 = ((bf16[128,8,256]{2,0,1:T(8,128)(2,1)}), bf16[128,8,256]{2,0,1:T(8,128)(2,1)S(1)}, u32[]{:S(2)}, u32[]{:S(2)}) async-start(bf16[128,8,256]{2,0,1:T(8,128)(2,1)} %bitcast.73), calls=%async_computation.2 | async-start | bytes 1048576 | tf_op jit(solution)/shard_map/all_to_all | solution.py:111
  328.1 6.0 %copy-start.13 = (bf16[128,2048]{1,0:T(8,128)(2,1)S(1)}, bf16[128,2048]{1,0:T(8,128)(2,1)}, u32[]{:S(2)}) copy-start(bf16[128,2048]{1,0:T(8,128)(2,1)} %copy-done.11) | copy-start | bytes 1572868
  328.1 251.6 %all-gather.43.cloned.1.call-start = ((), (), s32[]{:S(2)}) async-start(), calls=%async_computation.19 | async-start | bytes 2621440 | tf_op jit(solution)/shard_map/all_gather | solution.py:23
  334.0 2.1 copy-start.8
  334.0 30.9 %copy-start.6 = (bf16[128,2048]{1,0:T(8,128)(2,1)S(1)}, bf16[128,2048]{1,0:T(8,128)(2,1)}, u32[]{:S(2)}) copy-start(bf16[128,2048]{1,0:T(8,128)(2,1)} %param.19) | copy-start | bytes 1572868
  366.3 66.6 %all-to-all-start = ((bf16[128,8,256]{2,0,1:T(8,128)(2,1)}), bf16[128,8,256]{2,0,1:T(8,128)(2,1)S(1)}, u32[]{:S(2)}, u32[]{:S(2)}) async-start(bf16[128,8,256]{2,0,1:T(8,128)(2,1)} %bitcast.63), calls=%async_computation | async-start | bytes 1048576 | tf_op jit(solution)/shard_map/all_to_all | solution.py:111
  374.5 55.7 %copy-start.17 = (f32[256,704]{0,1:T(8,128)S(1)}, f32[256,704]{0,1:T(8,128)}, u32[]{:S(2)}) copy-start(f32[256,704]{0,1:T(8,128)} %param.34) | copy-start | bytes 2162692
  433.0 59.6 %copy-start.18 = (f32[256,704]{0,1:T(8,128)S(1)}, f32[256,704]{0,1:T(8,128)}, u32[]{:S(2)}) copy-start(f32[256,704]{0,1:T(8,128)} %param.30) | copy-start | bytes 2162692
  433.0 88.8 %all-to-all-start.1 = ((bf16[128,8,256]{2,0,1:T(8,128)(2,1)}), bf16[128,8,256]{2,0,1:T(8,128)(2,1)S(1)}, u32[]{:S(2)}, u32[]{:S(2)}) async-start(bf16[128,8,256]{2,0,1:T(8,128)(2,1)} %bitcast.62), calls=%async_computation.1 | async-start | bytes 1048576 | tf_op jit(solution)/shard_map/all_to_all | solution.py:112
  468.9 50.2 %copy-start.19 = (f32[256,704]{0,1:T(8,128)S(1)}, f32[256,704]{0,1:T(8,128)}, u32[]{:S(2)}) copy-start(f32[256,704]{0,1:T(8,128)} %param.31) | copy-start | bytes 2162692
  495.3 50.2 %copy-start.20 = (f32[704,256]{1,0:T(8,128)S(1)}, f32[704,256]{1,0:T(8,128)}, u32[]{:S(2)}) copy-start(f32[704,256]{1,0:T(8,128)} %param.32) | copy-start | bytes 2162692
Sparse Core Ops, SparseCore 0:
  9.6 37.1 all-gather.26
  48.4 35.2 all-gather.22
  85.3 35.2 all-gather.24
  122.0 35.2 all-gather.16
  158.7 35.2 all-gather.18
  195.4 35.2 all-gather.20
  234.3 44.0 all-reduce.2
  280.8 35.5 all-gather.40
  319.9 45.0 all-reduce.4
  366.4 35.4 all-gather.34
  403.5 26.6 all-gather.36
  432.2 33.6 all-gather.38
  467.5 24.9 all-gather.28
  494.0 24.9 all-gather.30
  520.5 24.9 all-gather.32
  547.8 31.8 all-gather.42
